TPU v7x, 32 devices: a whole 2x2x4 slice. The times are simulated.
32 devices in a mesh: grp: 2 (over y), ep: 4 (over z), tp: 4 (over x, core).
Axes of the slice: x: 2, y: 2, z: 4, core: 2. Of those that a mesh axis runs over, the one named last changes fastest.
Arguments:
- tokens: bfloat16 [48, 2048], P('grp', 'ep'), parts along dimension 0, may hold values from -70 to 70
- first_gain: float32 [2048], replicated, may hold values from 0.1 to 1.9
- w_query: bfloat16 [2048, 2048], P('ep', 'tp'), may hold values from -0.125 to 0.125
- w_key: bfloat16 [2048, 2048], P('ep', 'tp'), may hold values from -0.125 to 0.125
- w_value: bfloat16 [2048, 4096], P('ep', 'tp'), may hold values from -0.125 to 0.125
- w_outgate: bfloat16 [2048, 4096], P('ep', 'tp'), may hold values from -0.125 to 0.125
- w_input: bfloat16 [2048, 16], replicated, may hold values from -0.125 to 0.125
- w_forget: bfloat16 [2048, 16], replicated, may hold values from -0.125 to 0.125
- input_bias: float32 [16], replicated, may hold values from -3 to 3
- forget_bias: float32 [16], replicated, may hold values from -2 to 5
- head_gain: float32 [4096], replicated, may hold values from 0.1 to 1.9
- w_project: bfloat16 [4096, 2048], P('tp', 'ep'), may hold values from -0.09375 to 0.09375
- cell_state: float32 [48, 16, 128, 256], P(('grp', 'ep'), 'tp'), parts along dimension 0, may hold values from -6 to 6
- norm_state: float32 [48, 16, 128], P(('grp', 'ep'), 'tp'), parts along dimension 0, may hold values from -6 to 6
- max_state: float32 [48, 16], P(('grp', 'ep'), 'tp'), parts along dimension 0, may hold values from -110 to 110
- second_gain: float32 [2048], replicated, may hold values from 0.1 to 1.9
- routes: int32 [48, 2], P('grp'), parts along dimension 0, may hold values from 0 to 3, all different within a row; in each aligned block of 6 rows (0 to 5, 6 to 11, ...) at most 6 rows name the same one
- route_weight: float32 [48, 2], P('grp'), parts along dimension 0, may hold values from 0.2 to 1
- expert_gate: bfloat16 [4, 2048, 4096], P('ep', None, 'tp'), may hold values from -0.125 to 0.125
- expert_up: bfloat16 [4, 2048, 4096], P('ep', None, 'tp'), may hold values from -0.125 to 0.125
- expert_down: bfloat16 [4, 4096, 2048], P('ep', 'tp'), may hold values from -0.09375 to 0.09375
Outputs:
- layer_out: bfloat16 [48, 2048], P('grp', 'ep'), parts along dimension 0
- new_cell: float32 [48, 16, 128, 256], P(('grp', 'ep'), 'tp'), parts along dimension 0
- new_norm: float32 [48, 16, 128], P(('grp', 'ep'), 'tp'), parts along dimension 0
- new_max: float32 [48, 16], P(('grp', 'ep'), 'tp'), parts along dimension 0
There are 2 independent parts, one for each index of `grp`. A program takes and returns all parts, laid end to end along the dimension named above; an argument that names none is the same for every part. Nothing has to cross between parts.
Inputs may be any that keep to these rules, and one draw needn't show every extreme that they name: `routes`: each sequence names 2 different experts. In each aligned block of 6 sequences no expert is named by more than 6 of them, a bound that some block reaches.
All inputs are finite; a program needn't handle non-finite values.
Results may differ from a plain program's by a relative error of at most 0.0065.
Values may be sent and summed in bfloat16 or wider, within the bound.
A program may use at most 64 MiB of HBM per device.

v0:
```python
import jax
import jax.numpy as jnp
from jax import lax
from jax.sharding import PartitionSpec as P

EXP_DEV = 1


NORM_EPS = 1e-05
HEAD_EPS = 1e-06


def row_norm(stream_rows, gain_whole):
    col_count = stream_rows.shape[1]
    gain_cols = lax.dynamic_slice_in_dim(gain_whole, lax.axis_index("ep") * col_count, col_count, 0)
    values = stream_rows.astype(jnp.float32)
    totals, squares = lax.psum((jnp.sum(values, axis=1), jnp.sum(values * values, axis=1)), "ep")
    features = col_count * lax.axis_size("ep")
    row_mean = totals / features
    spread = squares / features - row_mean * row_mean
    inv_scale = lax.rsqrt(spread + NORM_EPS)
    return ((values - row_mean[:, None]) * inv_scale[:, None] * gain_cols).astype(jnp.bfloat16)


def expert_act(gate_sum, up_sum):
    return (jax.nn.silu(gate_sum) * up_sum).astype(jnp.bfloat16)


def scatter_slots(active, expert_down):
    slot_major = jnp.moveaxis(active, 1, 0)
    return lax.psum_scatter(
        jnp.einsum(
            "pef,efd->ped", slot_major, expert_down, preferred_element_type=jnp.float32
        ).astype(jnp.bfloat16),
        "tp",
        scatter_dimension=0,
        tiled=True,
    )


def on_device(
    tokens,
    first_gain,
    w_query,
    w_key,
    w_value,
    w_outgate,
    w_input,
    w_forget,
    input_bias,
    forget_bias,
    head_gain,
    w_project,
    cell_state,
    norm_state,
    max_state,
    second_gain,
    routes,
    route_weight,
    expert_gate,
    expert_up,
    expert_down,
):
    blocks = lax.axis_size("ep")
    columns = tokens.shape[1]
    seq_total = tokens.shape[0]
    seq_local = seq_total // blocks
    heads_local = cell_state.shape[1]
    key_size = cell_state.shape[2]
    value_size = cell_state.shape[3]
    col_start = lax.axis_index("ep") * columns
    head_start = lax.axis_index("tp") * heads_local
    normed = row_norm(tokens, first_gain)
    input_cols = lax.dynamic_slice(w_input, (col_start, head_start), (columns, heads_local))
    forget_cols = lax.dynamic_slice(w_forget, (col_start, head_start), (columns, heads_local))

    def project_part(weight):
        return jnp.dot(normed, weight, preferred_element_type=jnp.float32)

    summed = (
        lax.psum_scatter(project_part(w_query), "ep", scatter_dimension=0, tiled=True),
        lax.psum_scatter(project_part(w_key), "ep", scatter_dimension=0, tiled=True),
        lax.psum_scatter(project_part(w_value), "ep", scatter_dimension=0, tiled=True),
        lax.psum_scatter(project_part(w_outgate), "ep", scatter_dimension=0, tiled=True),
        lax.psum_scatter(project_part(input_cols), "ep", scatter_dimension=0, tiled=True),
        lax.psum_scatter(project_part(forget_cols), "ep", scatter_dimension=0, tiled=True),
    )
    queries = summed[0].astype(jnp.bfloat16).reshape(seq_local, heads_local, key_size)
    key_rows = summed[1].astype(jnp.bfloat16).reshape(seq_local, heads_local, key_size)
    value_rows = summed[2].astype(jnp.bfloat16).reshape(seq_local, heads_local, value_size)
    outgate = summed[3].astype(jnp.bfloat16)
    input_pre = summed[4] + lax.dynamic_slice_in_dim(input_bias, head_start, heads_local, 0)
    forget_pre = summed[5] + lax.dynamic_slice_in_dim(forget_bias, head_start, heads_local, 0)
    carried = jax.nn.log_sigmoid(forget_pre) + max_state
    new_max = jnp.maximum(carried, input_pre)
    keep_old = jnp.exp(carried - new_max)
    admit_new = jnp.exp(input_pre - new_max)
    key_float = key_rows.astype(jnp.float32)
    value_float = value_rows.astype(jnp.float32)
    new_cell = (
        keep_old[:, :, None, None] * cell_state
        + admit_new[:, :, None, None] * key_float[:, :, :, None] * value_float[:, :, None, :]
    )
    new_norm = keep_old[:, :, None] * norm_state + admit_new[:, :, None] * key_float
    query_float = queries.astype(jnp.float32) * key_size ** (-0.5)
    readout = jnp.einsum("shk,shkv->shv", query_float, new_cell, precision=lax.Precision.HIGHEST)
    head_mean = jnp.mean(readout, axis=2, keepdims=True)
    centred = readout - head_mean
    head_var = jnp.mean(centred * centred, axis=2, keepdims=True)
    gains_here = lax.dynamic_slice_in_dim(
        head_gain, head_start * value_size, heads_local * value_size, 0
    )
    mixed_heads = (
        (centred * lax.rsqrt(head_var + HEAD_EPS)).reshape(seq_local, heads_local * value_size)
        * gains_here
        * jax.nn.sigmoid(outgate.astype(jnp.float32))
    ).astype(jnp.bfloat16)
    head_terms = jnp.dot(
        lax.all_gather(mixed_heads, "ep", axis=0, tiled=True),
        w_project,
        preferred_element_type=jnp.float32,
    )
    mixer_out = lax.psum(head_terms, "tp")
    stream = (tokens.astype(jnp.float32) + mixer_out).astype(jnp.bfloat16)
    second_normed = row_norm(stream, second_gain)
    experts = blocks * EXP_DEV
    top_count = routes.shape[1]
    capacity = max(2, 2 * seq_local * top_count // experts)
    slot_count = blocks * capacity
    expert_ids = lax.broadcasted_iota(jnp.int32, (1, 1, experts), 2)
    matches = routes[:, :, None] == expert_ids
    routed = jnp.sum(matches.astype(jnp.int32), axis=1)
    combine = jnp.sum(jnp.where(matches, route_weight[:, :, None], 0.0), axis=1)
    running = (
        jnp.cumsum(routed.reshape(blocks, seq_local, experts), axis=1).reshape(seq_total, experts)
        - routed
    )
    block_ids = lax.broadcasted_iota(jnp.int32, (seq_total, experts), 0) // seq_local
    slot_of = block_ids * capacity + running
    slot_ids = lax.broadcasted_iota(jnp.int32, (experts, slot_count, seq_total), 1)
    placed = (slot_of.T[:, None, :] == slot_ids) & (routed.T[:, None, :] > 0)
    picker = placed.astype(jnp.bfloat16)
    weighted = jnp.where(placed, combine.T[:, None, :], 0.0)
    mine_pick = lax.dynamic_slice_in_dim(picker, lax.axis_index("ep") * EXP_DEV, EXP_DEV, 0)
    mine_weight = lax.dynamic_slice_in_dim(weighted, lax.axis_index("ep") * EXP_DEV, EXP_DEV, 0)
    chosen = jnp.einsum(
        "eps,sd->epd",
        mine_pick,
        lax.all_gather(second_normed, "ep", axis=1, tiled=True),
        preferred_element_type=jnp.float32,
    ).astype(jnp.bfloat16)
    gate_part = jnp.einsum("epd,edf->epf", chosen, expert_gate, preferred_element_type=jnp.float32)
    up_part = jnp.einsum("epd,edf->epf", chosen, expert_up, preferred_element_type=jnp.float32)
    active = expert_act(gate_part, up_part)
    share = scatter_slots(active, expert_down)
    every_slot = lax.all_gather(share, "tp", axis=0, tiled=True)
    spread_terms = jnp.einsum(
        "eps,ped->sd", mine_weight, every_slot.astype(jnp.float32), precision=lax.Precision.HIGHEST
    )
    moe_out = lax.psum_scatter(
        spread_terms.astype(jnp.bfloat16), "ep", scatter_dimension=1, tiled=True
    ).astype(jnp.float32)
    layer_out = (stream.astype(jnp.float32) + moe_out).astype(jnp.bfloat16)
    return (layer_out, new_cell, new_norm, new_max)


def solution(mesh):
    placed = (
        P("grp", "ep"),
        P(),
        P("ep", "tp"),
        P("ep", "tp"),
        P("ep", "tp"),
        P("ep", "tp"),
        P(),
        P(),
        P(),
        P(),
        P(),
        P("tp", "ep"),
        P(("grp", "ep"), "tp", None, None),
        P(("grp", "ep"), "tp", None),
        P(("grp", "ep"), "tp"),
        P(),
        P("grp", None),
        P("grp", None),
        P("ep", None, "tp"),
        P("ep", None, "tp"),
        P("ep", "tp", None),
    )
    return jax.shard_map(
        on_device,
        mesh=mesh,
        in_specs=placed,
        out_specs=(
            P("grp", "ep"),
            P(("grp", "ep"), "tp", None, None),
            P(("grp", "ep"), "tp", None),
            P(("grp", "ep"), "tp"),
        ),
        check_vma=False,
    )
```

profile of v0, /device:TPU:0, one launch (start us, length us, event | category | flops | bytes accessed | tf_op | source)
XLA Modules:
  0.0 173.8 jit_solution(15154943931951436978)
XLA Ops:
  7.2 0.0 copy-start
  7.2 0.0 copy-start.8
  7.2 0.0 copy-start.6
  7.3 0.0 reduce-scatter.15.cloned.1.call-start
  7.3 1.0 convert_reduce_fusion.1
  8.3 0.8 dynamic_slice.27
  9.0 13.5 %all-reduce.14 = (f32[24]{0:T(128)S(1)}, f32[24]{0:T(128)S(1)}) all-reduce(f32[24]{0:T(128)S(1)} %get-tuple-element.7, f32[24]{0:T(128)S(1)} %get-tuple-element.6), channel_id=1, replica_groups=mesh['grp'=2,'ep'=4,'tp'=4] {'ep'}, use_global_device_ids=true, to_apply=%region_3.0 | all-reduce | flops 48 | bytes 384 | tf_op jit(solution)/shard_map/psum | solution.py:17
  22.5 0.8 fusion.34
  23.3 0.3 fusion.72
  23.6 1.5 fusion.74
  25.1 1.2 fusion.70
  26.3 1.2 fusion.71
  27.5 11.9 %fusion.66 = (f32[8,1024]{1,0:T(8,128)S(1)}, f32[8,512]{1,0:T(8,128)S(1)}, f32[8,1024]{1,0:T(8,128)S(1)}, f32[8,512]{1,0:T(8,128)S(1)}) fusion(f32[24,1024]{1,0:T(8,128)S(1)} %fusion.74, f32[24,512]{1,0:T(8,128)S(1)} %fusion.70, f32[24,1024]{1,0:T(8,128)S(1)} %fusion.72, f32[24,512]{1,0:T(8,128)S(1)} %fusion.71), kind=kCustom, calls=%all-reduce-scatter.5 | all-reduce-scatter fusion | flops 98305 | bytes 393728
  39.5 3.7 %collective-permute-start.1 = (bf16[6,512]{1,0:T(8,128)(2,1)S(1)}, bf16[6,512]{1,0:T(8,128)(2,1)S(1)}, u32[]{:S(2)}, u32[]{:S(2)}) collective-permute-start(bf16[6,512]{1,0:T(8,128)(2,1)S(1)} %slice.1), channel_id=1, source_target_pairs={{0,4},{4,8},{8,12},{1,5},{5,9},{9,13},{2,6},{6,10},{10,14},{3,7},{... | collective-permute-start | bytes 18440
  43.2 1.9 %collective-permute-start.2 = (bf16[6,1024]{1,0:T(8,128)(2,1)S(1)}, bf16[6,1024]{1,0:T(8,128)(2,1)S(1)}, u32[]{:S(2)}, u32[]{:S(2)}) collective-permute-start(bf16[6,1024]{1,0:T(8,128)(2,1)S(1)} %slice.2), channel_id=1, source_target_pairs={{0,4},{4,8},{8,12},{1,5},{5,9},{9,13},{2,6},{6,10},{10,14},{3,7},{... | collective-permute-start | bytes 36872
  45.2 3.4 %collective-permute-start = (bf16[6,512]{1,0:T(8,128)(2,1)S(1)}, bf16[6,512]{1,0:T(8,128)(2,1)S(1)}, u32[]{:S(2)}, u32[]{:S(2)}) collective-permute-start(bf16[6,512]{1,0:T(8,128)(2,1)S(1)} %slice), channel_id=1, source_target_pairs={{0,4},{4,8},{8,12},{1,5},{5,9},{9,13},{2,6},{6,10},{10,14},{3,7},{... | collective-permute-start | bytes 18440
  48.6 1.9 %collective-permute-start.3 = (bf16[6,1024]{1,0:T(8,128)(2,1)S(1)}, bf16[6,1024]{1,0:T(8,128)(2,1)S(1)}, u32[]{:S(2)}, u32[]{:S(2)}) collective-permute-start(bf16[6,1024]{1,0:T(8,128)(2,1)S(1)} %slice.3), channel_id=1, source_target_pairs={{0,4},{4,8},{8,12},{1,5},{5,9},{9,13},{2,6},{6,10},{10,14},{3,7},{... | collective-permute-start | bytes 36872
  50.5 0.7 convert_reduce_fusion.2
  51.2 0.1 reshape.111
  51.3 0.9 fusion.54
  52.2 0.9 fusion.56
  53.1 0.1 dynamic_slice.31
  53.2 0.1 dynamic_slice.29
  53.2 0.6 fusion.69
  53.8 8.3 %all-reduce.13 = (f32[24,4]{0,1:T(4,128)S(1)}, f32[24,4]{0,1:T(4,128)S(1)}) all-reduce(f32[24,4]{0,1:T(4,128)S(1)} %fusion.56, f32[24,4]{0,1:T(4,128)S(1)} %fusion.54), channel_id=3, replica_groups=mesh['grp'=2,'ep'=4,'tp'=4] {'ep'}, use_global_device_ids=true, to_apply=%region_5.0.clone | all-reduce | flops 192 | bytes 1536
  62.9 0.1 subtract_exponential_fusion.1
  63.0 0.1 subtract_exponential_fusion
  63.0 0.7 reduce_window_sum.11
  63.7 0.1 reshape.112
  64.5 0.1 copy.48
  64.6 0.1 copy.47
  64.7 0.8 dynamic_slice.35
  65.5 0.1 concatenate.1
  65.6 0.7 multiply_add_fusion.1
  66.3 0.1 concatenate
  66.5 0.1 concatenate.2
  66.6 0.0 dynamic-slice-start
  66.7 2.5 %multiply_add_fusion = f32[6,4,128,256]{3,2,1,0:T(8,128)S(1)} fusion(f32[6,4,128,256]{3,2,1,0:T(8,128)} %param.33, f32[6,4,256]{2,1,0:T(4,128)S(1)} %reshape.120, f32[6,4,128]{2,1,0:T(4,128)S(1)} %get-tuple-element.23, f32[6,4]{1,0:T(8,128)S(1)} %copy.47), kind=kLoop, calls=%fused_computation.6 | loop fusion | flops 2359296 | bytes 6328416 | tf_op jit(solution)/shard_map/add | solution.py:101
  69.2 0.0 copy-start.1
  69.2 1.7 copy-done.1
  70.9 1.6 fusion.73
  72.5 0.1 bitcast_reduce_fusion
  72.6 0.2 multiply_reduce_fusion
  72.7 0.1 multiply_bitcast_fusion
  72.9 0.1 concatenate.3
  73.0 13.1 %all-gather = bf16[4,6,1024]{2,1,0:T(8,128)(2,1)S(1)} all-gather(bf16[1,6,1024]{2,1,0:T(8,128)(2,1)S(1)} %fusion.45), channel_id=1, replica_groups=mesh['grp'=2,'ep'=4,'tp'=4] {'ep'}, dimensions={0}, use_global_device_ids=true | all-gather | bytes 61440 | tf_op jit(solution)/shard_map/all_gather | solution.py:119
  86.2 0.2 fusion.75
  86.4 10.5 %psum.37 = f32[24,512]{1,0:T(8,128)S(1)} all-reduce(f32[24,512]{1,0:T(8,128)S(1)} %fusion.75), channel_id=1, replica_groups=mesh['grp'=2,'ep'=4,'tp'=4] {'tp'}, use_global_device_ids=true, to_apply=%region_12.13 | all-reduce | flops 12288 | bytes 98304 | tf_op jit(solution)/shard_map/psum | solution.py:123
  97.0 0.1 convert_reduce_fusion
  97.1 10.4 %all-reduce.12 = (f32[24]{0:T(128)S(1)}, f32[24]{0:T(128)S(1)}) all-reduce(f32[24]{0:T(128)S(1)} %get-tuple-element.5, f32[24]{0:T(128)S(1)} %get-tuple-element.4), channel_id=1, replica_groups=mesh['grp'=2,'ep'=4,'tp'=4] {'ep'}, use_global_device_ids=true, to_apply=%region_19.20 | all-reduce | flops 48 | bytes 384 | tf_op jit(solution)/shard_map/psum | solution.py:17
  107.5 0.1 fusion.39
  107.6 13.3 %all_gather.10 = bf16[24,2048]{1,0:T(8,128)(2,1)S(1)} all-gather(bf16[24,512]{1,0:T(8,128)(2,1)S(1)} %fusion.39), channel_id=1, replica_groups=mesh['grp'=2,'ep'=4,'tp'=4] {'ep'}, dimensions={1}, use_global_device_ids=true | all-gather | bytes 122880 | tf_op jit(solution)/shard_map/all_gather | solution.py:149
  120.9 0.2 convolution_convert_fusion.1
  121.0 2.9 %fusion.9 = f32[24,1024]{1,0:T(8,128)S(1)} fusion(bf16[24,2048]{1,0:T(8,128)(2,1)S(1)} %convolution_convert_fusion.1, bf16[1,2048,1024]{2,1,0:T(8,128)(2,1)} %param.39), kind=kOutput, calls=%fused_computation.4 | convolution fusion | flops 100663296 | bytes 4390912 | tf_op jit(solution)/shard_map/epd,edf->epf/dot_general | solution.py:152
  123.9 4.7 %fusion.14 = bf16[24,1,2048]{2,0,1:T(8,128)(2,1)S(1)} fusion(bf16[1,1024,2048]{2,1,0:T(8,128)(2,1)} %param.41, bf16[24,2048]{1,0:T(8,128)(2,1)S(1)} %convolution_convert_fusion.1, bf16[1,2048,1024]{2,1,0:T(8,128)(2,1)} %param.40, f32[24,1024]{1,0:T(8,128)S(1)} %fusion.9), kind=kOutput, calls=%fused_computation.10 | convolution fusion | flops 201523200 | bytes 8683520 | tf_op jit(solution)/shard_map/pef,efd->ped/dot_general | solution.py:32
  128.6 8.3 %fusion.4 = bf16[8,2048]{1,0:T(8,128)(2,1)S(1)} fusion(bf16[24,1,2048]{2,0,1:T(8,128)(2,1)S(1)} %fusion.14), kind=kCustom, calls=%all-reduce-scatter.4 | all-reduce-scatter fusion | flops 65537 | bytes 131584
  136.9 1.3 collective-permute-start.4
  138.3 0.6 dynamic-slice.33
  139.5 0.2 concatenate.4
  139.8 6.9 %all_gather.11 = bf16[24,1,2048]{2,1,0:T(2,128)(2,1)S(1)} all-gather(bf16[6,1,2048]{2,1,0:T(2,128)(2,1)S(1)} %copy.49), channel_id=1, replica_groups=mesh['grp'=2,'ep'=4,'tp'=4] {'tp'}, dimensions={0}, use_global_device_ids=true | all-gather | bytes 122880 | tf_op jit(solution)/shard_map/all_gather | solution.py:156
  146.7 0.9 convolution_convert_fusion
  147.6 0.0 reduce-scatter.15.cloned.1.call-update
  147.6 18.0 %reduce-scatter.15.cloned.1.call-done = bf16[24,512]{1,0:T(8,128)(2,1)} async-done(((bf16[24,2048]{1,0:T(8,128)(2,1)}), bf16[24,512]{1,0:T(8,128)(2,1)}) %reduce-scatter.15.cloned.1.call-update) | async-done | bytes 24592 | tf_op jit(solution)/shard_map/reduce_scatter | solution.py:160
  165.6 1.4 fusion.41
  (54 shorter events, 0.5 us)
Async XLA Ops:
  7.2 16.2 %copy-start = (bf16[512,1024]{1,0:T(8,128)(2,1)S(1)}, bf16[512,1024]{1,0:T(8,128)(2,1)}, u32[]{:S(2)}) copy-start(bf16[512,1024]{1,0:T(8,128)(2,1)} %param.25) | copy-start | bytes 3145732
  7.2 46.1 %copy-start.8 = (u32[32]{0:T(128)S(1)}, u32[32]{0:T(128)}, u32[]{:S(2)}) copy-start(u32[32]{0:T(128)} %constant.70) | copy-start | bytes 388
  7.2 56.7 %copy-start.6 = (s32[24,2]{0,1:T(2,128)S(1)}, s32[24,2]{0,1:T(2,128)}, u32[]{:S(2)}) copy-start(s32[24,2]{0,1:T(2,128)} %param.37) | copy-start | bytes 580
  7.2 45.9 %copy-start.11 = (f32[16]{0:T(128)S(1)}, f32[16]{0:T(128)}, u32[]{:S(2)}) copy-start(f32[16]{0:T(128)} %param.29) | copy-start | bytes 196
  7.2 46.0 %copy-start.12 = (f32[16]{0:T(128)S(1)}, f32[16]{0:T(128)}, u32[]{:S(2)}) copy-start(f32[16]{0:T(128)} %param.30) | copy-start | bytes 196
  7.2 55.6 %copy-start.7 = (f32[6,4]{0,1:T(4,128)S(1)}, f32[6,4]{0,1:T(4,128)}, u32[]{:S(2)}) copy-start(f32[6,4]{0,1:T(4,128)} %param.35) | copy-start | bytes 292
  7.2 56.6 %copy-start.9 = (f32[24,2]{0,1:T(2,128)S(1)}, f32[24,2]{0,1:T(2,128)}, u32[]{:S(2)}) copy-start(f32[24,2]{0,1:T(2,128)} %param.38) | copy-start | bytes 580
  7.2 58.4 %copy-start.4 = (f32[6,4,128]{2,1,0:T(4,128)S(1)}, f32[6,4,128]{2,1,0:T(4,128)}, u32[]{:S(2)}) copy-start(f32[6,4,128]{2,1,0:T(4,128)} %param.34) | copy-start | bytes 36868
  7.3 158.3 %reduce-scatter.15.cloned.1.call-start = ((), (), s32[]{:S(2)}) async-start(), calls=%async_computation.1 | async-start | bytes 122880 | tf_op jit(solution)/shard_map/reduce_scatter | solution.py:160
  39.5 26.0 %collective-permute-start.1 = (bf16[6,512]{1,0:T(8,128)(2,1)S(1)}, bf16[6,512]{1,0:T(8,128)(2,1)S(1)}, u32[]{:S(2)}, u32[]{:S(2)}) collective-permute-start(bf16[6,512]{1,0:T(8,128)(2,1)S(1)} %slice.1), channel_id=1, source_target_pairs={{0,4},{4,8},{8,12},{1,5},{5,9},{9,13},{2,6},{6,10},{10,14},{3,7},{... | collective-permute-start | bytes 18440
  43.2 23.2 %collective-permute-start.2 = (bf16[6,1024]{1,0:T(8,128)(2,1)S(1)}, bf16[6,1024]{1,0:T(8,128)(2,1)S(1)}, u32[]{:S(2)}, u32[]{:S(2)}) collective-permute-start(bf16[6,1024]{1,0:T(8,128)(2,1)S(1)} %slice.2), channel_id=1, source_target_pairs={{0,4},{4,8},{8,12},{1,5},{5,9},{9,13},{2,6},{6,10},{10,14},{3,7},{... | collective-permute-start | bytes 36872
  45.2 21.2 %collective-permute-start = (bf16[6,512]{1,0:T(8,128)(2,1)S(1)}, bf16[6,512]{1,0:T(8,128)(2,1)S(1)}, u32[]{:S(2)}, u32[]{:S(2)}) collective-permute-start(bf16[6,512]{1,0:T(8,128)(2,1)S(1)} %slice), channel_id=1, source_target_pairs={{0,4},{4,8},{8,12},{1,5},{5,9},{9,13},{2,6},{6,10},{10,14},{3,7},{... | collective-permute-start | bytes 18440
  48.6 24.3 %collective-permute-start.3 = (bf16[6,1024]{1,0:T(8,128)(2,1)S(1)}, bf16[6,1024]{1,0:T(8,128)(2,1)S(1)}, u32[]{:S(2)}, u32[]{:S(2)}) collective-permute-start(bf16[6,1024]{1,0:T(8,128)(2,1)S(1)} %slice.3), channel_id=1, source_target_pairs={{0,4},{4,8},{8,12},{1,5},{5,9},{9,13},{2,6},{6,10},{10,14},{3,7},{... | collective-permute-start | bytes 36872
  62.9 9.5 %copy-start.5 = (f32[6,4]{0,1:T(4,128)}, f32[6,4]{0,1:T(4,128)S(1)}, u32[]{:S(2)}) copy-start(f32[6,4]{0,1:T(4,128)S(1)} %get-tuple-element.26) | copy-start | bytes 292
  66.6 6.4 %dynamic-slice-start = ((f32[4096]{0:T(1024)}, s32[]{:T(128)}), f32[1024]{0:T(1024)S(1)}, s32[]{:S(2)}) async-start(f32[4096]{0:T(1024)} %param.31, s32[]{:T(128)} %select_n.40), calls=%async_computation.2 | async-start | bytes 8704 | tf_op jit(solution)/shard_map/dynamic_slice | solution.py:110
  66.6 19.5 %copy-start.2 = (bf16[1024,512]{1,0:T(8,128)(2,1)S(1)}, bf16[1024,512]{1,0:T(8,128)(2,1)}, u32[]{:S(2)}) copy-start(bf16[1024,512]{1,0:T(8,128)(2,1)} %param.32) | copy-start | bytes 3145732
  66.7 30.3 %copy-start.3 = (bf16[24,512]{1,0:T(8,128)(2,1)S(1)}, bf16[24,512]{1,0:T(8,128)(2,1)}, u32[]{:S(2)}) copy-start(bf16[24,512]{1,0:T(8,128)(2,1)} %param.21) | copy-start | bytes 73732
  69.2 1.7 copy-start.1
  123.9 14.4 %copy-start.10 = (u32[32]{0:T(128)S(1)}, u32[32]{0:T(128)}, u32[]{:S(2)}) copy-start(u32[32]{0:T(128)} %constant.94) | copy-start | bytes 388
  136.9 2.6 %collective-permute-start.4 = (bf16[6,2048]{1,0:T(8,128)(2,1)S(1)}, bf16[6,2048]{1,0:T(8,128)(2,1)S(1)}, u32[]{:S(2)}, u32[]{:S(2)}) collective-permute-start(bf16[6,2048]{1,0:T(8,128)(2,1)S(1)} %slice.4), channel_id=1, source_target_pairs={{0,1},{1,2},{2,3},{4,5},{5,6},{6,7},{8,9},{9,10},{10,11},{12,13},{... | collective-permute-start | bytes 73736
Sparse Core Ops, SparseCore 0:
  147.7 17.8 reduce-scatter.14
where the time goes:
time: 175 us; the launch traced here: 174 us
  blocking collectives  96.3 us (55%)
  waiting for transfers between devices  18 us (10%)
  between operations  16.5 us (9%)
  matrix products  16.4 us (9%)
  starting transfers between devices  12.3 us (7%)
  other arithmetic  8.63 us (5%)
  local copies, waits for them, and re-layouts  5.68 us (3%)
    unnamed x3, blocking collectives  28.6 us
    psum x2, blocking collectives, row_norm(): lax.psum((jnp.sum(values, axis=1), jnp.sum(values * values, axis=1)), 'ep')  23.8 us
    reduce_scatter x1, waiting for transfers between devices, on_device(): lax.psum_scatter(spread_terms.astype(jnp.bfloat16), 'ep', scatter_dimensi...  18 us
    all_gather x1, blocking collectives, on_device(): lax.all_gather(second_normed, 'ep', axis=1, tiled=True)  13.3 us
    all_gather x1, blocking collectives, on_device(): lax.all_gather(mixed_heads, 'ep', axis=0, tiled=True)  13.1 us
    unnamed x5, starting transfers between devices  12.2 us
    psum x1, blocking collectives, on_device(): mixer_out = lax.psum(head_terms, 'tp')  10.5 us
    all_gather x1, blocking collectives, on_device(): every_slot = lax.all_gather(share, 'tp', axis=0, tiled=True)  6.92 us
  transfers between devices with their start and end apart: 6, of which 1 were waited for; matrix products, arithmetic and copies ran while one was open for 7% of the time, Pallas kernels for 0%

commit v1 on v0

v1 whole, which is shorter than its diff:
```python
import functools

import jax
import jax.numpy as jnp
from jax import lax
from jax.experimental import pallas as pl
from jax.experimental.pallas import tpu as pltpu
from jax.sharding import PartitionSpec as P

NORM_EPS = 1e-05
HEAD_EPS = 1e-06
F32 = jnp.float32
BF16 = jnp.bfloat16
MESH = pl.DeviceIdType.MESH


def each(start, stop, body):
    if stop - start <= 16:
        for index in range(start, stop):
            body(index)
    else:
        lax.fori_loop(start, stop, lambda index, none: (body(index), none)[1], 0)


def tiles(width, body, most=256):
    size = min(width, most)
    if width == size:
        body(0, size)
    else:
        def step(index, none):
            body(pl.multiple_of(index * size, size), size)
            return none

        lax.fori_loop(0, width // size, step, 0)


def layer_kernel(
    E, T, SB, PB,
    tokens, first_gain, w_input, w_forget, input_bias, forget_bias, head_gain,
    norm_state, max_state, second_gain, routes, route_weight,
    w_query, w_key, w_value, w_outgate, w_project, cell_state, gate_w, up_w, down_w,
    layer_out, new_norm, new_max, key_out, value_out, keep_out,
    wall, wproj, cell, gate, up, down,
    tok_all, tok_pad, normed, pre_gate, proj_send, proj_recv, rows_out,
    mix_rows, mix_all, mix_mat, term_send, term_recv, stream_all, second, act,
    exp_send, exp_recv, final_send, final_recv, weight_rows, out_rows,
    load_sem, s0, r0, s1, r1, s2, r2, s3, r3, s4, r4, s5, r5, s6, r6,
):
    e = lax.axis_index("ep")
    t = lax.axis_index("tp")
    G = E * T
    S, C = tokens.shape
    SP = E * PB
    Hl, DK = norm_state.shape[1], norm_state.shape[2]
    DV = cell_state.shape[3]
    QW, VW = Hl * DK, Hl * DV

    loads = []
    starts = (
        (w_query, wall.at[:, 0:QW]),
        (w_key, wall.at[:, QW : 2 * QW]),
        (w_value, wall.at[:, 2 * QW : 2 * QW + VW]),
        (w_outgate, wall.at[:, 2 * QW + VW : 2 * QW + 2 * VW]),
        (cell_state, cell),
        (w_project, wproj),
        (gate_w.at[0], gate),
        (up_w.at[0], up),
        (down_w.at[0], down),
    )
    for number, (source, target) in enumerate(starts):
        loads.append(pltpu.make_async_copy(source, target, load_sem.at[number]))
        loads[-1].start()

    barrier = pltpu.get_barrier_semaphore()

    def peer(d):
        return lax.rem(e + d // T, E), lax.rem(t + d % T, T)

    def behind(d):
        return lax.rem(e + E - d // T, E), lax.rem(t + T - d % T, T)

    def greet(d):
        pe, pt = peer(d)
        pl.semaphore_signal(barrier, inc=1, device_id={"ep": pe, "tp": pt}, device_id_type=MESH)

    each(1, G, greet)
    pl.semaphore_wait(barrier, G - 1)

    def ep_copy(d, source, target, ss, rs):
        return pltpu.make_async_remote_copy(
            src_ref=source, dst_ref=target, send_sem=ss.at[d], recv_sem=rs.at[d],
            device_id={"ep": lax.rem(e + d, E)}, device_id_type=MESH,
        )

    def tp_copy(d, source, target, ss, rs):
        return pltpu.make_async_remote_copy(
            src_ref=source, dst_ref=target, send_sem=ss.at[d], recv_sem=rs.at[d],
            device_id={"tp": lax.rem(t + d, T)}, device_id_type=MESH,
        )

    def all_copy(d, source, target, ss, rs):
        pe, pt = peer(d)
        return pltpu.make_async_remote_copy(
            src_ref=source, dst_ref=target, send_sem=ss.at[d], recv_sem=rs.at[d],
            device_id={"ep": pe, "tp": pt}, device_id_type=MESH,
        )

    each(1, E, lambda d: ep_copy(d, tokens, tok_all.at[e], s0, r0).start())
    tok_all[e] = tokens[...]

    row = lax.broadcasted_iota(jnp.int32, (SP, S), 0)
    col = lax.broadcasted_iota(jnp.int32, (SP, S), 1)
    spread_f = jnp.where(((row // PB) * SB + row % PB == col) & (row % PB < SB), 1.0, 0.0).astype(F32)
    spread = spread_f.astype(BF16)
    weight = jnp.sum(jnp.where(routes[...] == e, route_weight[...], 0.0), axis=1, keepdims=True)
    weight = jnp.broadcast_to(weight, (S, 128))
    weight_rows[...] = jnp.dot(
        spread_f, weight, precision=lax.Precision.HIGHEST, preferred_element_type=F32
    ).reshape(E, PB, 128)

    each(1, E, lambda d: ep_copy(d, tokens, tok_all.at[lax.rem(e + E - d, E)], s0, r0).wait_recv())
    total = jnp.zeros((SP, 1), F32)
    square = jnp.zeros((SP, 1), F32)
    for b in range(E):
        x = jnp.dot(spread, tok_all[b], preferred_element_type=F32)
        tok_pad[b] = x
        total = total + jnp.sum(x, axis=1, keepdims=True)
        square = square + jnp.sum(x * x, axis=1, keepdims=True)
    mean = total / (E * C)
    inv = lax.rsqrt(square / (E * C) - mean * mean + NORM_EPS)
    for b in range(E):
        normed[b] = ((tok_pad[b] - mean) * inv * first_gain[b : b + 1, :]).astype(BF16)

    for load in loads[:4]:
        load.wait()

    mine = normed[e]

    def project(at, size):
        part = jnp.dot(mine, wall[:, pl.ds(at, size)], preferred_element_type=F32)
        proj_send[:, :, pl.ds(at, size)] = part.reshape(E, PB, size)

    tiles(wall.shape[1], project)

    def send_proj(d):
        ep_copy(d, proj_send.at[lax.rem(e + d, E)], proj_recv.at[e], s1, r1).start()

    each(1, E, send_proj)
    proj_recv[e] = proj_send[e]

    pre_i = jnp.zeros((SP, w_input.shape[1]), F32)
    pre_f = jnp.zeros((SP, w_input.shape[1]), F32)
    for b in range(E):
        pre_i = pre_i + jnp.dot(normed[b], w_input[b * C : (b + 1) * C, :], preferred_element_type=F32)
        pre_f = pre_f + jnp.dot(normed[b], w_forget[b * C : (b + 1) * C, :], preferred_element_type=F32)
    pre_gate[0] = (pre_i + input_bias[...]).reshape(E, PB, w_input.shape[1])
    pre_gate[1] = (pre_f + forget_bias[...]).reshape(E, PB, w_input.shape[1])
    my_i = pre_gate[0, e][:SB]
    my_f = pre_gate[1, e][:SB]
    lane = lax.broadcasted_iota(jnp.int32, my_i.shape, 1)
    keeps, admits = [], []
    for h in range(Hl):
        i_col = jnp.sum(jnp.where(lane == t * Hl + h, my_i, 0.0), axis=1, keepdims=True)
        f_col = jnp.sum(jnp.where(lane == t * Hl + h, my_f, 0.0), axis=1, keepdims=True)
        log_sig = jnp.minimum(f_col, 0.0) - jnp.log1p(jnp.exp(-jnp.abs(f_col)))
        carried = log_sig + max_state[:, h : h + 1]
        top = jnp.maximum(carried, i_col)
        keep = jnp.exp(carried - top)
        new_max[:, h : h + 1] = top
        keep_out[:, h : h + 1] = keep
        keeps.append(keep)
        admits.append(jnp.exp(i_col - top))
    mix_rows[...] = jnp.zeros_like(mix_rows)
    loads[4].wait()

    each(1, E, lambda d: ep_copy(d, proj_send.at[0], proj_recv.at[lax.rem(e + E - d, E)], s1, r1).wait_recv())
    summed = proj_recv[0]
    for b in range(1, E):
        summed = summed + proj_recv[b]
    rounded = summed.astype(BF16).astype(F32)
    gains = head_gain[pl.ds(t, 1), :]
    for h in range(Hl):
        q8 = rounded[:, h * DK : (h + 1) * DK] * (DK ** -0.5)
        k = rounded[:SB, QW + h * DK : QW + (h + 1) * DK]
        v = rounded[:SB, 2 * QW + h * DV : 2 * QW + (h + 1) * DV]
        gate_o = rounded[:SB, 2 * QW + VW + h * DV : 2 * QW + VW + (h + 1) * DV]
        turned = q8.T
        for s in range(SB):
            rows_out[s : s + 1, :] = jnp.sum(
                turned[:, s : s + 1] * cell[s, h], axis=0, keepdims=True
            )
        q_k = jnp.sum(q8[:SB] * k, axis=1, keepdims=True)
        read = keeps[h] * rows_out[0:SB, :] + (admits[h] * q_k) * v
        centred = read - jnp.mean(read, axis=1, keepdims=True)
        var = jnp.mean(centred * centred, axis=1, keepdims=True)
        mix_rows[0:SB, h * DV : (h + 1) * DV] = (
            centred * lax.rsqrt(var + HEAD_EPS) * gains[:, h * DV : (h + 1) * DV]
            * jax.nn.sigmoid(gate_o)
        )
        admitted = admits[h] * k
        key_out[:, h, :] = admitted
        value_out[:, h, :] = v
        new_norm[:, h, :] = keeps[h] * norm_state[:, h, :] + admitted
    mix_all[e] = mix_rows[...].astype(BF16)

    each(1, E, lambda d: ep_copy(d, mix_all.at[e], mix_all.at[e], s2, r2).start())
    loads[5].wait()
    each(1, E, lambda d: ep_copy(d, mix_all.at[e], mix_all.at[lax.rem(e + E - d, E)], s2, r2).wait_recv())
    mix_mat[...] = mix_all[...].astype(F32).reshape(SP, VW).astype(BF16)

    def out_project(at, size):
        part = jnp.dot(mix_mat[...], wproj[:, pl.ds(at, size)], preferred_element_type=F32)
        term_send[:, :, pl.ds(at, size)] = part.reshape(T, PB, size)

    tiles(C, out_project)
    each(1, T, lambda d: tp_copy(d, term_send.at[lax.rem(t + d, T)], term_recv.at[t], s3, r3).start())
    term_recv[t] = term_send[t]
    out_rows[...] = tok_pad[e].reshape(E, PB, C)
    each(1, T, lambda d: tp_copy(d, term_send.at[0], term_recv.at[lax.rem(t + T - d, T)], s3, r3).wait_recv())
    mixer = term_recv[0]
    for b in range(1, T):
        mixer = mixer + term_recv[b]
    stream_all[e, t] = (out_rows[t] + mixer).astype(BF16)

    each(1, G, lambda d: all_copy(d, stream_all.at[e, t], stream_all.at[e, t], s4, r4).start())

    def take_stream(d):
        be, bt = behind(d)
        all_copy(d, stream_all.at[e, t], stream_all.at[be, bt], s4, r4).wait_recv()

    for load in loads[6:8]:
        load.wait()
    each(1, G, take_stream)
    total = jnp.zeros((SP, 1), F32)
    square = jnp.zeros((SP, 1), F32)
    for b in range(E):
        x = stream_all[b].astype(F32).reshape(SP, C)
        tok_pad[b] = x
        total = total + jnp.sum(x, axis=1, keepdims=True)
        square = square + jnp.sum(x * x, axis=1, keepdims=True)
    mean = total / (E * C)
    inv = lax.rsqrt(square / (E * C) - mean * mean + NORM_EPS)
    for b in range(E):
        second[:, b * C : (b + 1) * C] = (
            (tok_pad[b] - mean) * inv * second_gain[b : b + 1, :]
        ).astype(BF16)

    def hidden(at, size):
        g = jnp.dot(second[...], gate[:, pl.ds(at, size)], preferred_element_type=F32)
        u = jnp.dot(second[...], up[:, pl.ds(at, size)], preferred_element_type=F32)
        act[:, pl.ds(at, size)] = (g * jax.nn.sigmoid(g) * u).astype(BF16)

    tiles(gate.shape[1], hidden)
    loads[8].wait()

    def lower(at, size):
        part = jnp.dot(act[...], down[:, pl.ds(at, size)], preferred_element_type=F32)
        exp_send[:, :, pl.ds(at, size)] = part.reshape(T, PB, size).astype(BF16)

    tiles(down.shape[1], lower)
    each(1, T, lambda d: tp_copy(d, exp_send.at[lax.rem(t + d, T)], exp_recv.at[t], s5, r5).start())
    exp_recv[t] = exp_send[t]
    each(1, T, lambda d: tp_copy(d, exp_send.at[0], exp_recv.at[lax.rem(t + T - d, T)], s5, r5).wait_recv())
    whole = exp_recv[0].astype(F32)
    for b in range(1, T):
        whole = whole + exp_recv[b].astype(F32)
    weighted = whole.astype(BF16).astype(F32) * weight_rows[t][:, 0:1]
    for b in range(E):
        final_send[b] = weighted[:, b * C : (b + 1) * C].astype(BF16)

    def send_final(d):
        pe, pt = peer(d)
        all_copy(d, final_send.at[pe], final_recv.at[e, t], s6, r6).start()

    each(1, G, send_final)
    final_recv[e, t] = final_send[e]

    def take_final(d):
        be, bt = behind(d)
        all_copy(d, final_send.at[0], final_recv.at[be, bt], s6, r6).wait_recv()

    each(1, G, take_final)
    moe = final_recv[0].astype(F32)
    for b in range(1, E):
        moe = moe + final_recv[b].astype(F32)
    done = (tok_pad[e] + moe.reshape(SP, C)).astype(BF16)
    back_row = lax.broadcasted_iota(jnp.int32, (S, SP), 0)
    back_col = lax.broadcasted_iota(jnp.int32, (S, SP), 1)
    gather = jnp.where((back_row // SB) * PB + back_row % SB == back_col, 1.0, 0.0).astype(BF16)
    layer_out[...] = jnp.dot(gather, done, preferred_element_type=F32).astype(BF16)

    each(1, E, lambda d: ep_copy(d, tokens, tok_all.at[e], s0, r0).wait_send())
    each(1, E, lambda d: ep_copy(d, proj_send.at[0], proj_recv.at[e], s1, r1).wait_send())
    each(1, E, lambda d: ep_copy(d, mix_all.at[e], mix_all.at[e], s2, r2).wait_send())
    each(1, T, lambda d: tp_copy(d, term_send.at[0], term_recv.at[t], s3, r3).wait_send())
    each(1, G, lambda d: all_copy(d, stream_all.at[e, t], stream_all.at[e, t], s4, r4).wait_send())
    each(1, T, lambda d: tp_copy(d, exp_send.at[0], exp_recv.at[t], s5, r5).wait_send())
    each(1, G, lambda d: all_copy(d, final_send.at[0], final_recv.at[e, t], s6, r6).wait_send())


def on_device(
    E, T,
    tokens, first_gain, w_query, w_key, w_value, w_outgate, w_input, w_forget,
    input_bias, forget_bias, head_gain, w_project, cell_state, norm_state, max_state,
    second_gain, routes, route_weight, expert_gate, expert_up, expert_down,
):
    S, C = tokens.shape
    SB, Hl, DK, DV = cell_state.shape
    D = first_gain.shape[0]
    FL = expert_gate.shape[2]
    PB = -(-SB // 8) * 8
    SP = E * PB
    heads = w_input.shape[1]
    width = 2 * Hl * (DK + DV)
    VW = Hl * DV
    vmem = pl.BlockSpec(memory_space=pltpu.VMEM)
    hbm = pl.BlockSpec(memory_space=pl.ANY)
    V = pltpu.VMEM
    dma = pltpu.SemaphoreType.DMA
    G = E * T
    layer_out, new_norm, new_max, admitted, values, keep = pl.pallas_call(
        functools.partial(layer_kernel, E, T, SB, PB),
        out_shape=(
            jax.ShapeDtypeStruct((S, C), BF16),
            jax.ShapeDtypeStruct((SB, Hl, DK), F32),
            jax.ShapeDtypeStruct((SB, Hl), F32),
            jax.ShapeDtypeStruct((SB, Hl, DK), F32),
            jax.ShapeDtypeStruct((SB, Hl, DV), F32),
            jax.ShapeDtypeStruct((SB, Hl), F32),
        ),
        in_specs=[vmem] * 12 + [hbm] * 9,
        out_specs=(vmem,) * 6,
        scratch_shapes=[
            V((C, width), BF16),
            V(w_project.shape, BF16),
            V(cell_state.shape, F32),
            V((D, FL), BF16),
            V((D, FL), BF16),
            V((FL, D), BF16),
            V((E, S, C), BF16),
            V((E, SP, C), F32),
            V((E, SP, C), BF16),
            V((2, E, PB, heads), F32),
            V((E, PB, width), F32),
            V((E, PB, width), F32),
            V((PB, DV), F32),
            V((PB, VW), F32),
            V((E, PB, VW), BF16),
            V((SP, VW), BF16),
            V((T, PB, C), F32),
            V((T, PB, C), F32),
            V((E, T, PB, C), BF16),
            V((SP, D), BF16),
            V((SP, FL), BF16),
            V((T, PB, D), BF16),
            V((T, PB, D), BF16),
            V((E, PB, C), BF16),
            V((E, T, PB, C), BF16),
            V((E, PB, 128), F32),
            V((E, PB, C), F32),
            dma((9,)),
            dma((E,)), dma((E,)), dma((E,)), dma((E,)), dma((E,)), dma((E,)),
            dma((T,)), dma((T,)), dma((G,)), dma((G,)), dma((T,)), dma((T,)),
            dma((G,)), dma((G,)),
        ],
        compiler_params=pltpu.CompilerParams(
            collective_id=0, has_side_effects=True, vmem_limit_bytes=56 * 1024 * 1024
        ),
        name="layer",
    )(
        tokens, first_gain.reshape(E, C), w_input, w_forget,
        input_bias.reshape(1, heads), forget_bias.reshape(1, heads),
        head_gain.reshape(T, VW), norm_state, max_state, second_gain.reshape(E, C),
        routes, route_weight,
        w_query, w_key, w_value, w_outgate, w_project, cell_state,
        expert_gate, expert_up, expert_down,
    )
    new_cell = (
        keep[:, :, None, None] * cell_state + admitted[:, :, :, None] * values[:, :, None, :]
    )
    return layer_out, new_cell, new_norm, new_max


def solution(mesh):
    placed = (
        P("grp", "ep"), P(), P("ep", "tp"), P("ep", "tp"), P("ep", "tp"), P("ep", "tp"),
        P(), P(), P(), P(), P(), P("tp", "ep"),
        P(("grp", "ep"), "tp", None, None), P(("grp", "ep"), "tp", None), P(("grp", "ep"), "tp"),
        P(), P("grp", None), P("grp", None),
        P("ep", None, "tp"), P("ep", None, "tp"), P("ep", "tp", None),
    )
    return jax.shard_map(
        functools.partial(on_device, mesh.shape["ep"], mesh.shape["tp"]),
        mesh=mesh,
        in_specs=placed,
        out_specs=(
            P("grp", "ep"),
            P(("grp", "ep"), "tp", None, None),
            P(("grp", "ep"), "tp", None),
            P(("grp", "ep"), "tp"),
        ),
        check_vma=False,
    )
```

time: 175 us -> 68.9 us (0.39)
  blocking collectives: 96.3 us -> 0 us
  Pallas kernels: 0 us -> 50.6 us
  waiting for transfers between devices: 18 us -> 0 us
  matrix products: 16.4 us -> 0 us
  between operations: 16.5 us -> 0.65 us
  starting transfers between devices: 12.3 us -> 0 us
  local copies, waits for them, and re-layouts: 5.68 us -> 14.2 us
  other arithmetic: 8.63 us -> 2.96 us
    pallas_call x0 -> x1, Pallas kernels: none -> 50.6 us  [on_device(): pl.pallas_call(functools.partial(layer_kernel, E, T, SB, PB), out_shape=(...]
    psum x3 -> x0, blocking collectives: 34.4 us -> none  [the longest x2 23.8 us: row_norm(): lax.psum((jnp.sum(values, axis=1), jnp.sum(values * values, axis=1)), 'ep')]
    all_gather x3 -> x0, blocking collectives: 33.3 us -> none  [the longest x1 13.3 us: on_device(): lax.all_gather(second_normed, 'ep', axis=1, tiled=True)]
    unnamed x3 -> x0, blocking collectives: 28.6 us -> none
    reduce_scatter x1 -> x0, waiting for transfers between devices: 18 us -> none  [on_device(): lax.psum_scatter(spread_terms.astype(jnp.bfloat16), 'ep', scatter_dimensi...]
    dot_general x12 -> x0, matrix products: 16.4 us -> none  [the longest x6 5.96 us: project_part(): return jnp.dot(normed, weight, preferred_element_type=jnp.float32)]
    unnamed x5 -> x0, starting transfers between devices: 12.2 us -> none
    unnamed x41 -> x14, local copies, waits for them, and re-layouts: 3.55 us -> 10.3 us
  transfers between devices with their start and end apart: 6 -> 0, of which waited for: 1 -> 0; matrix products, arithmetic and copies ran while one was open for 7% -> 0% of each run, Pallas kernels for 0% -> 0%
where the time goes in v1:
time: 68.9 us; the launch traced here: 68.4 us
  Pallas kernels  50.6 us (73%)
  local copies, waits for them, and re-layouts  14.2 us (21%)
  other arithmetic  2.96 us (4%)
    pallas_call x1, Pallas kernels, on_device(): pl.pallas_call(functools.partial(layer_kernel, E, T, SB, PB), out_shape=(...  50.6 us
    unnamed x14, local copies, waits for them, and re-layouts  10.3 us
    add x1, other arithmetic, on_device(): keep[:, :, None, None] * cell_state  2.96 us

profile of v1, /device:TPU:0, one launch (start us, length us, event | category | flops | bytes accessed | tf_op | source)
XLA Modules:
  0.0 68.4 jit_solution(15037518796821359311)
XLA Ops:
  0.6 1.4 %copy.27.max_state = f32[6,4]{1,0:T(8,128)} copy(f32[6,4]{0,1:T(4,128)} %param.35) | data formatting | bytes 192 | tf_op args[14]
  2.0 1.3 %reshape.26.first_gain = f32[4,512]{1,0:T(4,128)} reshape(f32[2048]{0:T(1024)} %param.22) | data formatting | bytes 16384 | tf_op jit(solution)/shard_map/reshape | solution.py:371
  3.3 1.3 %reshape.30.second_gain = f32[4,512]{1,0:T(4,128)} reshape(f32[2048]{0:T(1024)} %param.36) | data formatting | bytes 16384 | tf_op jit(solution)/shard_map/reshape | solution.py:373
  4.6 1.4 %copy.28.routes = s32[24,2]{1,0:T(8,128)} copy(s32[24,2]{0,1:T(2,128)} %param.37) | data formatting | bytes 384 | tf_op args[16]
  5.9 1.3 %copy.29.route_weight = f32[24,2]{1,0:T(8,128)} copy(f32[24,2]{0,1:T(2,128)} %param.38) | data formatting | bytes 384 | tf_op args[17]
  7.3 1.3 %reshape.29.head_gain = f32[4,1024]{1,0:T(4,128)} reshape(f32[4096]{0:T(1024)} %param.31) | data formatting | bytes 32768 | tf_op jit(solution)/shard_map/reshape | solution.py:373
  8.6 1.8 %copy.25.w_input = bf16[2048,16]{1,0:T(8,128)(2,1)} copy(bf16[2048,16]{0,1:T(8,128)(2,1)} %param.27) | data formatting | bytes 131072 | tf_op args[6]
  10.5 1.8 %copy.26.w_forget = bf16[2048,16]{1,0:T(8,128)(2,1)} copy(bf16[2048,16]{0,1:T(8,128)(2,1)} %param.28) | data formatting | bytes 131072 | tf_op args[7]
  12.3 0.0 copy-start
  12.3 50.6 %layer.1 = (bf16[24,512]{1,0:T(8,128)(2,1)}, f32[6,4,128]{2,1,0:T(4,128)}, f32[6,4]{1,0:T(8,128)}, f32[6,4,128]{2,1,0:T(4,128)}, f32[6,4,256]{2,1,0:T(4,128)}, /*index=5*/f32[6,4]{1,0:T(8,128)}) custom-call(bf16[24,512]{1,0:T(8,128)(2,1)} %tokens.1, f32[4,512]{1,0:T(4,128)} %reshape.26.first_gain, bf16[2048,16]{1,0:T(8,128)(2,1)} %copy.25.w_input, ...), custom_call_target="tpu_custom_call" | custom-call | tf_op jit(solution)/shard_map/layer/pallas_call | solution.py:321
  62.9 1.3 %copy.30 = f32[6,4]{0,1:T(4,128)} copy(f32[6,4]{1,0:T(8,128)} %get-tuple-element.19) | data formatting | bytes 192
  64.2 0.0 copy-done
  64.2 0.0 copy-start.1
  64.2 0.0 copy-start.2
  64.2 3.0 %multiply_add_fusion = f32[6,4,128,256]{3,2,1,0:T(8,128)} fusion(f32[6,4,128,256]{3,2,1,0:T(8,128)S(1)} %copy-done, f32[6,4,256]{2,1,0:T(4,128)} %get-tuple-element.13, f32[6,4,128]{2,1,0:T(4,128)} %get-tuple-element.12, f32[6,4]{1,0:T(8,128)} %get-tuple-element.11), kind=kLoop, calls=%fused_computation | loop fusion | flops 2359296 | bytes 6328416 | tf_op jit(solution)/shard_map/add | solution.py:379
  67.2 0.0 copy-done.1
  67.2 0.6 copy.33
  67.8 0.0 copy-done.2
  67.8 0.6 copy.34
Async XLA Ops:
  12.3 51.9 %copy-start = (f32[6,4,128,256]{3,2,1,0:T(8,128)S(1)}, f32[6,4,128,256]{3,2,1,0:T(8,128)}, u32[]{:S(2)}) copy-start(f32[6,4,128,256]{3,2,1,0:T(8,128)} %cell_state.1) | copy-start | bytes 9437188
  64.2 3.0 %copy-start.1 = (bf16[24,512]{1,0:T(8,128)(2,1)S(1)}, bf16[24,512]{1,0:T(8,128)(2,1)}, u32[]{:S(2)}) copy-start(bf16[24,512]{1,0:T(8,128)(2,1)} %get-tuple-element.24) | copy-start | bytes 73732
  64.2 3.6 %copy-start.2 = (f32[6,4,128]{2,1,0:T(4,128)S(1)}, f32[6,4,128]{2,1,0:T(4,128)}, u32[]{:S(2)}) copy-start(f32[6,4,128]{2,1,0:T(4,128)} %get-tuple-element.26) | copy-start | bytes 36868

commit v2 on v1

--- a/solution.py
+++ b/solution.py
@@ -23,7 +23,7 @@
 
 
 def tiles(width, body, most=256):
-    size = min(width, most)
+    size = next(s for s in (most, most // 2, width) if width % s == 0)
     if width == size:
         body(0, size)
     else:
@@ -41,7 +41,7 @@
     w_query, w_key, w_value, w_outgate, w_project, cell_state, gate_w, up_w, down_w,
     layer_out, new_norm, new_max, key_out, value_out, keep_out,
     wall, wproj, cell, gate, up, down,
-    tok_all, tok_pad, normed, pre_gate, proj_send, proj_recv, rows_out,
+    tok_all, tok_pad, normed, pre_gate, proj_own, proj_send, proj_recv, rows_out,
     mix_rows, mix_all, mix_mat, term_send, term_recv, stream_all, second, act,
     exp_send, exp_recv, final_send, final_recv, weight_rows, out_rows,
     load_sem, s0, r0, s1, r1, s2, r2, s3, r3, s4, r4, s5, r5, s6, r6,
@@ -71,6 +71,9 @@
         loads.append(pltpu.make_async_copy(source, target, load_sem.at[number]))
         loads[-1].start()
 
+    for landing in (term_recv, mix_all, stream_all, exp_recv, final_recv):
+        landing[...] = jnp.zeros_like(landing)
+
     barrier = pltpu.get_barrier_semaphore()
 
     def peer(d):
@@ -112,10 +115,9 @@
     col = lax.broadcasted_iota(jnp.int32, (SP, S), 1)
     spread_f = jnp.where(((row // PB) * SB + row % PB == col) & (row % PB < SB), 1.0, 0.0).astype(F32)
     spread = spread_f.astype(BF16)
-    weight = jnp.sum(jnp.where(routes[...] == e, route_weight[...], 0.0), axis=1, keepdims=True)
-    weight = jnp.broadcast_to(weight, (S, 128))
-    weight_rows[...] = jnp.dot(
-        spread_f, weight, precision=lax.Precision.HIGHEST, preferred_element_type=F32
+    weight = jnp.sum(jnp.where(routes[...] == e, route_weight[...], 0.0), axis=0, keepdims=True)
+    weight_rows[...] = jnp.broadcast_to(
+        jnp.sum(jnp.where(spread_f > 0.0, weight, 0.0), axis=1, keepdims=True), (SP, 128)
     ).reshape(E, PB, 128)
 
     each(1, E, lambda d: ep_copy(d, tokens, tok_all.at[lax.rem(e + E - d, E)], s0, r0).wait_recv())
@@ -129,56 +131,70 @@
     mean = total / (E * C)
     inv = lax.rsqrt(square / (E * C) - mean * mean + NORM_EPS)
     for b in range(E):
-        normed[b] = ((tok_pad[b] - mean) * inv * first_gain[b : b + 1, :]).astype(BF16)
+        normed[b] = ((tok_pad[b] - mean) * inv * first_gain[b * C : (b + 1) * C].reshape(1, C)).astype(BF16)
 
     for load in loads[:4]:
         load.wait()
 
     mine = normed[e]
 
-    def project(at, size):
-        part = jnp.dot(mine, wall[:, pl.ds(at, size)], preferred_element_type=F32)
-        proj_send[:, :, pl.ds(at, size)] = part.reshape(E, PB, size)
-
-    tiles(wall.shape[1], project)
-
-    def send_proj(d):
-        ep_copy(d, proj_send.at[lax.rem(e + d, E)], proj_recv.at[e], s1, r1).start()
-
-    each(1, E, send_proj)
-    proj_recv[e] = proj_send[e]
-
-    pre_i = jnp.zeros((SP, w_input.shape[1]), F32)
-    pre_f = jnp.zeros((SP, w_input.shape[1]), F32)
-    for b in range(E):
-        pre_i = pre_i + jnp.dot(normed[b], w_input[b * C : (b + 1) * C, :], preferred_element_type=F32)
-        pre_f = pre_f + jnp.dot(normed[b], w_forget[b * C : (b + 1) * C, :], preferred_element_type=F32)
-    pre_gate[0] = (pre_i + input_bias[...]).reshape(E, PB, w_input.shape[1])
-    pre_gate[1] = (pre_f + forget_bias[...]).reshape(E, PB, w_input.shape[1])
+    half = wall.shape[1] // 2
+
+    def proj_copy(d, part, source, slot):
+        cols = slice(part * half, (part + 1) * half)
+        return ep_copy(
+            d, proj_send.at[source, 0:SB, cols], proj_recv.at[slot, 0:SB, cols],
+            s1.at[part], r1.at[part],
+        )
+
+    for part in range(2):
+
+        def project(at, size, base=part * half):
+            at = pl.multiple_of(base + at, size)
+            total = jnp.dot(mine, wall[:, pl.ds(at, size)], preferred_element_type=F32)
+            total = total.reshape(E, PB, size)
+            proj_own[:, :, pl.ds(at, size)] = total
+            proj_send[:, :, pl.ds(at, size)] = total.astype(BF16)
+
+        tiles(half, project)
+        each(1, E, lambda d: proj_copy(d, part, lax.rem(e + d, E), e).start())
+
+    heads = w_input.shape[0]
+    pre_i = jnp.zeros((SP, heads), F32)
+    pre_f = jnp.zeros((SP, heads), F32)
+    across = (((1,), (1,)), ((), ()))
+    for b in range(E):
+        cols = slice(b * C, (b + 1) * C)
+        pre_i = pre_i + lax.dot_general(normed[b], w_input[:, cols], across, preferred_element_type=F32)
+        pre_f = pre_f + lax.dot_general(normed[b], w_forget[:, cols], across, preferred_element_type=F32)
+    pre_gate[0] = (pre_i + input_bias[...]).reshape(E, PB, heads)
+    pre_gate[1] = (pre_f + forget_bias[...]).reshape(E, PB, heads)
     my_i = pre_gate[0, e][:SB]
     my_f = pre_gate[1, e][:SB]
     lane = lax.broadcasted_iota(jnp.int32, my_i.shape, 1)
+    diag = lax.broadcasted_iota(jnp.int32, (SB, SB), 0) == lax.broadcasted_iota(jnp.int32, (SB, SB), 1)
     keeps, admits = [], []
     for h in range(Hl):
         i_col = jnp.sum(jnp.where(lane == t * Hl + h, my_i, 0.0), axis=1, keepdims=True)
         f_col = jnp.sum(jnp.where(lane == t * Hl + h, my_f, 0.0), axis=1, keepdims=True)
         log_sig = jnp.minimum(f_col, 0.0) - jnp.log1p(jnp.exp(-jnp.abs(f_col)))
-        carried = log_sig + max_state[:, h : h + 1]
+        carried = log_sig + jnp.sum(jnp.where(diag, max_state[h : h + 1, :], 0.0), axis=1, keepdims=True)
         top = jnp.maximum(carried, i_col)
         keep = jnp.exp(carried - top)
-        new_max[:, h : h + 1] = top
+        new_max[h : h + 1, :] = jnp.sum(jnp.where(diag, top, 0.0), axis=0, keepdims=True)
         keep_out[:, h : h + 1] = keep
         keeps.append(keep)
         admits.append(jnp.exp(i_col - top))
     mix_rows[...] = jnp.zeros_like(mix_rows)
     loads[4].wait()
 
-    each(1, E, lambda d: ep_copy(d, proj_send.at[0], proj_recv.at[lax.rem(e + E - d, E)], s1, r1).wait_recv())
-    summed = proj_recv[0]
-    for b in range(1, E):
-        summed = summed + proj_recv[b]
+    for part in range(2):
+        each(1, E, lambda d: proj_copy(d, part, 0, lax.rem(e + E - d, E)).wait_recv())
+    summed = proj_own[e]
+    for d in range(1, E):
+        summed = summed + proj_recv[lax.rem(e + E - d, E)].astype(F32)
     rounded = summed.astype(BF16).astype(F32)
-    gains = head_gain[pl.ds(t, 1), :]
+    gains = head_gain[pl.ds(pl.multiple_of(t * VW, VW), VW)].reshape(1, VW)
     for h in range(Hl):
         q8 = rounded[:, h * DK : (h + 1) * DK] * (DK ** -0.5)
         k = rounded[:SB, QW + h * DK : QW + (h + 1) * DK]
@@ -203,9 +219,9 @@
         new_norm[:, h, :] = keeps[h] * norm_state[:, h, :] + admitted
     mix_all[e] = mix_rows[...].astype(BF16)
 
-    each(1, E, lambda d: ep_copy(d, mix_all.at[e], mix_all.at[e], s2, r2).start())
+    each(1, E, lambda d: ep_copy(d, mix_all.at[e, 0:SB], mix_all.at[e, 0:SB], s2, r2).start())
     loads[5].wait()
-    each(1, E, lambda d: ep_copy(d, mix_all.at[e], mix_all.at[lax.rem(e + E - d, E)], s2, r2).wait_recv())
+    each(1, E, lambda d: ep_copy(d, mix_all.at[e, 0:SB], mix_all.at[lax.rem(e + E - d, E), 0:SB], s2, r2).wait_recv())
     mix_mat[...] = mix_all[...].astype(F32).reshape(SP, VW).astype(BF16)
 
     def out_project(at, size):
@@ -213,20 +229,20 @@
         term_send[:, :, pl.ds(at, size)] = part.reshape(T, PB, size)
 
     tiles(C, out_project)
-    each(1, T, lambda d: tp_copy(d, term_send.at[lax.rem(t + d, T)], term_recv.at[t], s3, r3).start())
+    each(1, T, lambda d: tp_copy(d, term_send.at[lax.rem(t + d, T), 0:SB], term_recv.at[t, 0:SB], s3, r3).start())
     term_recv[t] = term_send[t]
     out_rows[...] = tok_pad[e].reshape(E, PB, C)
-    each(1, T, lambda d: tp_copy(d, term_send.at[0], term_recv.at[lax.rem(t + T - d, T)], s3, r3).wait_recv())
+    each(1, T, lambda d: tp_copy(d, term_send.at[0, 0:SB], term_recv.at[lax.rem(t + T - d, T), 0:SB], s3, r3).wait_recv())
     mixer = term_recv[0]
     for b in range(1, T):
         mixer = mixer + term_recv[b]
     stream_all[e, t] = (out_rows[t] + mixer).astype(BF16)
 
-    each(1, G, lambda d: all_copy(d, stream_all.at[e, t], stream_all.at[e, t], s4, r4).start())
+    each(1, G, lambda d: all_copy(d, stream_all.at[e, t, 0:SB], stream_all.at[e, t, 0:SB], s4, r4).start())
 
     def take_stream(d):
         be, bt = behind(d)
-        all_copy(d, stream_all.at[e, t], stream_all.at[be, bt], s4, r4).wait_recv()
+        all_copy(d, stream_all.at[e, t, 0:SB], stream_all.at[be, bt, 0:SB], s4, r4).wait_recv()
 
     for load in loads[6:8]:
         load.wait()
@@ -242,7 +258,7 @@
     inv = lax.rsqrt(square / (E * C) - mean * mean + NORM_EPS)
     for b in range(E):
         second[:, b * C : (b + 1) * C] = (
-            (tok_pad[b] - mean) * inv * second_gain[b : b + 1, :]
+            (tok_pad[b] - mean) * inv * second_gain[b * C : (b + 1) * C].reshape(1, C)
         ).astype(BF16)
 
     def hidden(at, size):
@@ -253,14 +269,27 @@
     tiles(gate.shape[1], hidden)
     loads[8].wait()
 
-    def lower(at, size):
-        part = jnp.dot(act[...], down[:, pl.ds(at, size)], preferred_element_type=F32)
-        exp_send[:, :, pl.ds(at, size)] = part.reshape(T, PB, size).astype(BF16)
-
-    tiles(down.shape[1], lower)
-    each(1, T, lambda d: tp_copy(d, exp_send.at[lax.rem(t + d, T)], exp_recv.at[t], s5, r5).start())
+    mid = down.shape[1] // 2
+
+    def exp_copy(d, part, source, slot):
+        cols = slice(part * mid, (part + 1) * mid)
+        return tp_copy(
+            d, exp_send.at[source, 0:SB, cols], exp_recv.at[slot, 0:SB, cols],
+            s5.at[part], r5.at[part],
+        )
+
+    for part in range(2):
+
+        def lower(at, size, base=part * mid):
+            at = pl.multiple_of(base + at, size)
+            total = jnp.dot(act[...], down[:, pl.ds(at, size)], preferred_element_type=F32)
+            exp_send[:, :, pl.ds(at, size)] = total.reshape(T, PB, size).astype(BF16)
+
+        tiles(mid, lower)
+        each(1, T, lambda d: exp_copy(d, part, lax.rem(t + d, T), t).start())
     exp_recv[t] = exp_send[t]
-    each(1, T, lambda d: tp_copy(d, exp_send.at[0], exp_recv.at[lax.rem(t + T - d, T)], s5, r5).wait_recv())
+    for part in range(2):
+        each(1, T, lambda d: exp_copy(d, part, 0, lax.rem(t + T - d, T)).wait_recv())
     whole = exp_recv[0].astype(F32)
     for b in range(1, T):
         whole = whole + exp_recv[b].astype(F32)
@@ -270,14 +299,14 @@
 
     def send_final(d):
         pe, pt = peer(d)
-        all_copy(d, final_send.at[pe], final_recv.at[e, t], s6, r6).start()
+        all_copy(d, final_send.at[pe, 0:SB], final_recv.at[e, t, 0:SB], s6, r6).start()
 
     each(1, G, send_final)
     final_recv[e, t] = final_send[e]
 
     def take_final(d):
         be, bt = behind(d)
-        all_copy(d, final_send.at[0], final_recv.at[be, bt], s6, r6).wait_recv()
+        all_copy(d, final_send.at[0, 0:SB], final_recv.at[be, bt, 0:SB], s6, r6).wait_recv()
 
     each(1, G, take_final)
     moe = final_recv[0].astype(F32)
@@ -290,12 +319,14 @@
     layer_out[...] = jnp.dot(gather, done, preferred_element_type=F32).astype(BF16)
 
     each(1, E, lambda d: ep_copy(d, tokens, tok_all.at[e], s0, r0).wait_send())
-    each(1, E, lambda d: ep_copy(d, proj_send.at[0], proj_recv.at[e], s1, r1).wait_send())
-    each(1, E, lambda d: ep_copy(d, mix_all.at[e], mix_all.at[e], s2, r2).wait_send())
-    each(1, T, lambda d: tp_copy(d, term_send.at[0], term_recv.at[t], s3, r3).wait_send())
-    each(1, G, lambda d: all_copy(d, stream_all.at[e, t], stream_all.at[e, t], s4, r4).wait_send())
-    each(1, T, lambda d: tp_copy(d, exp_send.at[0], exp_recv.at[t], s5, r5).wait_send())
-    each(1, G, lambda d: all_copy(d, final_send.at[0], final_recv.at[e, t], s6, r6).wait_send())
+    for part in range(2):
+        each(1, E, lambda d: proj_copy(d, part, 0, e).wait_send())
+    each(1, E, lambda d: ep_copy(d, mix_all.at[e, 0:SB], mix_all.at[e, 0:SB], s2, r2).wait_send())
+    each(1, T, lambda d: tp_copy(d, term_send.at[0, 0:SB], term_recv.at[t, 0:SB], s3, r3).wait_send())
+    each(1, G, lambda d: all_copy(d, stream_all.at[e, t, 0:SB], stream_all.at[e, t, 0:SB], s4, r4).wait_send())
+    for part in range(2):
+        each(1, T, lambda d: exp_copy(d, part, 0, t).wait_send())
+    each(1, G, lambda d: all_copy(d, final_send.at[0, 0:SB], final_recv.at[e, t, 0:SB], s6, r6).wait_send())
 
 
 def on_device(
@@ -323,7 +354,7 @@
         out_shape=(
             jax.ShapeDtypeStruct((S, C), BF16),
             jax.ShapeDtypeStruct((SB, Hl, DK), F32),
-            jax.ShapeDtypeStruct((SB, Hl), F32),
+            jax.ShapeDtypeStruct((Hl, SB), F32),
             jax.ShapeDtypeStruct((SB, Hl, DK), F32),
             jax.ShapeDtypeStruct((SB, Hl, DV), F32),
             jax.ShapeDtypeStruct((SB, Hl), F32),
@@ -342,7 +373,8 @@
             V((E, SP, C), BF16),
             V((2, E, PB, heads), F32),
             V((E, PB, width), F32),
-            V((E, PB, width), F32),
+            V((E, PB, width), BF16),
+            V((E, PB, width), BF16),
             V((PB, DV), F32),
             V((PB, VW), F32),
             V((E, PB, VW), BF16),
@@ -359,8 +391,8 @@
             V((E, PB, 128), F32),
             V((E, PB, C), F32),
             dma((9,)),
-            dma((E,)), dma((E,)), dma((E,)), dma((E,)), dma((E,)), dma((E,)),
-            dma((T,)), dma((T,)), dma((G,)), dma((G,)), dma((T,)), dma((T,)),
+            dma((E,)), dma((E,)), dma((2, E)), dma((2, E)), dma((E,)), dma((E,)),
+            dma((T,)), dma((T,)), dma((G,)), dma((G,)), dma((2, T)), dma((2, T)),
             dma((G,)), dma((G,)),
         ],
         compiler_params=pltpu.CompilerParams(
@@ -368,17 +400,17 @@
         ),
         name="layer",
     )(
-        tokens, first_gain.reshape(E, C), w_input, w_forget,
+        tokens, first_gain, w_input.T, w_forget.T,
         input_bias.reshape(1, heads), forget_bias.reshape(1, heads),
-        head_gain.reshape(T, VW), norm_state, max_state, second_gain.reshape(E, C),
-        routes, route_weight,
+        head_gain, norm_state, max_state.T, second_gain,
+        routes.T, route_weight.T,
         w_query, w_key, w_value, w_outgate, w_project, cell_state,
         expert_gate, expert_up, expert_down,
     )
     new_cell = (
         keep[:, :, None, None] * cell_state + admitted[:, :, :, None] * values[:, :, None, :]
     )
-    return layer_out, new_cell, new_norm, new_max
+    return layer_out, new_cell, new_norm, new_max.T
 
 
 def solution(mesh):

time: 68.9 us -> 48.8 us (0.71)
  local copies, waits for them, and re-layouts: 14.2 us -> 1.8 us
  Pallas kernels: 50.6 us -> 43.2 us
    unnamed x14 -> x11, local copies, waits for them, and re-layouts: 10.3 us -> 1.8 us
    pallas_call x1, Pallas kernels: 50.6 us -> 43.2 us  [on_device(): pl.pallas_call(functools.partial(layer_kernel, E, T, SB, PB), out_shape=(...]
    reshape x3 -> x0, local copies, waits for them, and re-layouts: 3.93 us -> none  [the longest x1 1.33 us: on_device(): head_gain.reshape(T, VW)]
where the time goes in v2:
time: 48.8 us; the launch traced here: 48.6 us
  Pallas kernels  43.2 us (89%)
  other arithmetic  2.96 us (6%)
  local copies, waits for them, and re-layouts  1.8 us (4%)
  between operations  0.69 us (1%)
    pallas_call x1, Pallas kernels, on_device(): pl.pallas_call(functools.partial(layer_kernel, E, T, SB, PB), out_shape=(...  43.2 us
    add x1, other arithmetic, on_device(): keep[:, :, None, None] * cell_state  2.96 us
    unnamed x11, local copies, waits for them, and re-layouts  1.8 us

profile of v2, /device:TPU:0, one launch (start us, length us, event | category | flops | bytes accessed | tf_op | source)
XLA Modules:
  0.0 48.6 jit_solution(4508545327934978058)
XLA Ops:
  0.6 0.0 copy-start
  0.7 43.2 %layer.1 = (bf16[24,512]{1,0:T(8,128)(2,1)}, f32[6,4,128]{2,1,0:T(4,128)}, f32[4,6]{1,0:T(4,128)}, f32[6,4,128]{2,1,0:T(4,128)}, f32[6,4,256]{2,1,0:T(4,128)}, /*index=5*/f32[6,4]{1,0:T(8,128)}) custom-call(bf16[24,512]{1,0:T(8,128)(2,1)} %tokens.1, f32[2048]{0:T(1024)} %first_gain.1, bf16[16,2048]{1,0:T(8,128)(2,1)} %bitcast.8, bf16[16,2048]{1,0:T(8,128)(2,1)} %bitcast.9, ...), custom_call_target="tpu_custom_call" | custom-call | tf_op jit(solution)/shard_map/layer/pallas_call | solution.py:352
  43.8 0.0 copy-done
  43.8 0.0 copy-start.1
  43.9 0.0 copy-start.2
  43.9 0.0 copy-start.3
  43.9 3.0 %multiply_add_fusion = f32[6,4,128,256]{3,2,1,0:T(8,128)} fusion(f32[6,4,128,256]{3,2,1,0:T(8,128)S(1)} %copy-done, f32[6,4,256]{2,1,0:T(4,128)} %get-tuple-element.13, f32[6,4,128]{2,1,0:T(4,128)} %get-tuple-element.12, f32[6,4]{1,0:T(8,128)} %get-tuple-element.11), kind=kLoop, calls=%fused_computation | loop fusion | flops 2359296 | bytes 6328416 | tf_op jit(solution)/shard_map/add | solution.py:411
  46.8 0.0 copy-done.1
  46.8 0.6 %copy.28 = bf16[24,512]{1,0:T(8,128)(2,1)} copy(bf16[24,512]{1,0:T(8,128)(2,1)S(1)} %copy-done.1) | data formatting | bytes 49152
  47.4 0.0 copy-done.2
  47.4 0.6 %copy.29 = f32[6,4,128]{2,1,0:T(4,128)} copy(f32[6,4,128]{2,1,0:T(4,128)S(1)} %copy-done.2) | data formatting | bytes 24576
  48.0 0.0 copy-done.3
  48.0 0.6 %copy.30 = f32[6,4]{0,1:T(4,128)} copy(f32[6,4]{0,1:T(4,128)S(1)} %bitcast.11) | data formatting | bytes 192
Async XLA Ops:
  0.6 43.2 %copy-start = (f32[6,4,128,256]{3,2,1,0:T(8,128)S(1)}, f32[6,4,128,256]{3,2,1,0:T(8,128)}, u32[]{:S(2)}) copy-start(f32[6,4,128,256]{3,2,1,0:T(8,128)} %cell_state.1) | copy-start | bytes 9437188
  43.8 3.0 %copy-start.1 = (bf16[24,512]{1,0:T(8,128)(2,1)S(1)}, bf16[24,512]{1,0:T(8,128)(2,1)}, u32[]{:S(2)}) copy-start(bf16[24,512]{1,0:T(8,128)(2,1)} %get-tuple-element.20) | copy-start | bytes 73732
  43.9 3.6 %copy-start.2 = (f32[6,4,128]{2,1,0:T(4,128)S(1)}, f32[6,4,128]{2,1,0:T(4,128)}, u32[]{:S(2)}) copy-start(f32[6,4,128]{2,1,0:T(4,128)} %get-tuple-element.22) | copy-start | bytes 36868
  43.9 4.2 %copy-start.3 = (f32[4,6]{1,0:T(4,128)S(1)}, f32[4,6]{1,0:T(4,128)}, u32[]{:S(2)}) copy-start(f32[4,6]{1,0:T(4,128)} %get-tuple-element.15) | copy-start | bytes 292

commit v3 on v2

--- a/solution.py
+++ b/solution.py
@@ -193,7 +193,7 @@
     summed = proj_own[e]
     for d in range(1, E):
         summed = summed + proj_recv[lax.rem(e + E - d, E)].astype(F32)
-    rounded = summed.astype(BF16).astype(F32)
+    rounded = summed
     gains = head_gain[pl.ds(pl.multiple_of(t * VW, VW), VW)].reshape(1, VW)
     for h in range(Hl):
         q8 = rounded[:, h * DK : (h + 1) * DK] * (DK ** -0.5)

time: 48.8 us -> 48.8 us (level)
  no operation moved by 1% of the time
where the time goes in v3:
time: 48.8 us; the launch traced here: 48.6 us
  Pallas kernels  43.2 us (89%)
  other arithmetic  2.96 us (6%)
  local copies, waits for them, and re-layouts  1.8 us (4%)
  between operations  0.69 us (1%)
    pallas_call x1, Pallas kernels, on_device(): pl.pallas_call(functools.partial(layer_kernel, E, T, SB, PB), out_shape=(...  43.2 us
    add x1, other arithmetic, on_device(): keep[:, :, None, None] * cell_state  2.96 us
    unnamed x11, local copies, waits for them, and re-layouts  1.8 us

profile of v3, /device:TPU:0, one launch (start us, length us, event | category | flops | bytes accessed | tf_op | source)
XLA Modules:
  0.0 48.6 jit_solution(2483557569887989487)
XLA Ops:
  0.6 0.0 copy-start
  0.7 43.2 %layer.1 = (bf16[24,512]{1,0:T(8,128)(2,1)}, f32[6,4,128]{2,1,0:T(4,128)}, f32[4,6]{1,0:T(4,128)}, f32[6,4,128]{2,1,0:T(4,128)}, f32[6,4,256]{2,1,0:T(4,128)}, /*index=5*/f32[6,4]{1,0:T(8,128)}) custom-call(bf16[24,512]{1,0:T(8,128)(2,1)} %tokens.1, f32[2048]{0:T(1024)} %first_gain.1, bf16[16,2048]{1,0:T(8,128)(2,1)} %bitcast.8, bf16[16,2048]{1,0:T(8,128)(2,1)} %bitcast.9, ...), custom_call_target="tpu_custom_call" | custom-call | tf_op jit(solution)/shard_map/layer/pallas_call | solution.py:352
  43.8 0.0 copy-done
  43.8 0.0 copy-start.1
  43.9 0.0 copy-start.2
  43.9 0.0 copy-start.3
  43.9 3.0 %multiply_add_fusion = f32[6,4,128,256]{3,2,1,0:T(8,128)} fusion(f32[6,4,128,256]{3,2,1,0:T(8,128)S(1)} %copy-done, f32[6,4,256]{2,1,0:T(4,128)} %get-tuple-element.13, f32[6,4,128]{2,1,0:T(4,128)} %get-tuple-element.12, f32[6,4]{1,0:T(8,128)} %get-tuple-element.11), kind=kLoop, calls=%fused_computation | loop fusion | flops 2359296 | bytes 6328416 | tf_op jit(solution)/shard_map/add | solution.py:411
  46.8 0.0 copy-done.1
  46.8 0.6 %copy.28 = bf16[24,512]{1,0:T(8,128)(2,1)} copy(bf16[24,512]{1,0:T(8,128)(2,1)S(1)} %copy-done.1) | data formatting | bytes 49152
  47.4 0.0 copy-done.2
  47.4 0.6 %copy.29 = f32[6,4,128]{2,1,0:T(4,128)} copy(f32[6,4,128]{2,1,0:T(4,128)S(1)} %copy-done.2) | data formatting | bytes 24576
  48.0 0.0 copy-done.3
  48.0 0.6 %copy.30 = f32[6,4]{0,1:T(4,128)} copy(f32[6,4]{0,1:T(4,128)S(1)} %bitcast.11) | data formatting | bytes 192
Async XLA Ops:
  0.6 43.2 %copy-start = (f32[6,4,128,256]{3,2,1,0:T(8,128)S(1)}, f32[6,4,128,256]{3,2,1,0:T(8,128)}, u32[]{:S(2)}) copy-start(f32[6,4,128,256]{3,2,1,0:T(8,128)} %cell_state.1) | copy-start | bytes 9437188
  43.8 3.0 %copy-start.1 = (bf16[24,512]{1,0:T(8,128)(2,1)S(1)}, bf16[24,512]{1,0:T(8,128)(2,1)}, u32[]{:S(2)}) copy-start(bf16[24,512]{1,0:T(8,128)(2,1)} %get-tuple-element.20) | copy-start | bytes 73732
  43.9 3.6 %copy-start.2 = (f32[6,4,128]{2,1,0:T(4,128)S(1)}, f32[6,4,128]{2,1,0:T(4,128)}, u32[]{:S(2)}) copy-start(f32[6,4,128]{2,1,0:T(4,128)} %get-tuple-element.22) | copy-start | bytes 36868
  43.9 4.2 %copy-start.3 = (f32[4,6]{1,0:T(4,128)S(1)}, f32[4,6]{1,0:T(4,128)}, u32[]{:S(2)}) copy-start(f32[4,6]{1,0:T(4,128)} %get-tuple-element.15) | copy-start | bytes 292
